TPU v7x, 256 devices: a 4x2x16 block of a 4x16x16 slice. The times are simulated.
256 devices in a mesh: grp: 2 (over y), kv: 16 (over z), tp: 8 (over x, core).
Axes of the slice: x: 4, y: 2, z: 16, core: 2. Of those that a mesh axis runs over, the one named last changes fastest.
The devices are a block of a 4x16x16 slice.
Arguments:
- piece_tokens: bfloat16 [8192, 2048], P(('grp', 'kv')), parts along dimension 0, may hold values from -6 to 6
- dec_tokens: bfloat16 [128, 2048], P(('grp', 'kv')), parts along dimension 0, may hold values from -6 to 6
- norm_gain: float32 [2048], replicated, may hold values from 0.1 to 1.9
- query_weight: bfloat16 [2048, 1024], P(None, 'tp'), may hold values from -0.125 to 0.125
- key_weight: bfloat16 [2048, 1024], P(None, 'tp'), may hold values from -0.125 to 0.125
- value_weight: bfloat16 [2048, 1024], P(None, 'tp'), may hold values from -0.125 to 0.125
- forget_weight: bfloat16 [2048, 8], P(None, 'tp'), may hold values from -0.125 to 0.125
- forget_bias: float32 [8], P('tp'), may hold values from 3 to 13
- out_weight: bfloat16 [1024, 2048], P(None, 'tp'), may hold values from -0.1875 to 0.1875
- cache_keys: bfloat16 [131072, 1024], P(('grp', 'kv'), 'tp'), parts along dimension 0, may hold values from -480 to 480
- cache_values: bfloat16 [131072, 1024], P(('grp', 'kv'), 'tp'), parts along dimension 0, may hold values from -6 to 6
- cache_gates: float32 [8, 131072], P('tp', ('grp', 'kv')), parts along dimension 1, as said below
- dec_keys: bfloat16 [128, 2048, 1024], P(('grp', 'kv'), None, 'tp'), parts along dimension 0, may hold values from -480 to 480
- dec_values: bfloat16 [128, 2048, 1024], P(('grp', 'kv'), None, 'tp'), parts along dimension 0, may hold values from -6 to 6
- dec_gates: float32 [128, 8, 2048], P(('grp', 'kv'), 'tp'), parts along dimension 0, as said below
- dec_lengths: int32 [128], P(('grp', 'kv')), parts along dimension 0, may hold values from 1 to 2048, as said below
Outputs:
- piece_out: bfloat16 [8192, 2048], P(('grp', 'kv'), 'tp'), parts along dimension 0
- dec_out: bfloat16 [128, 2048], P(('grp', 'kv'), 'tp'), parts along dimension 0
- piece_keys: bfloat16 [8192, 1024], P(('grp', 'kv'), 'tp'), parts along dimension 0
- piece_values: bfloat16 [8192, 1024], P(('grp', 'kv'), 'tp'), parts along dimension 0
There are 2 independent parts, one for each index of `grp`. A program takes and returns all parts, laid end to end along the dimension named above; an argument that names none is the same for every part. Nothing has to cross between parts.
Inputs may be any that keep to these rules, and one draw needn't show every extreme that they name: cache_gates never falls along positions and is 0 at the last cached position. dec_gates never falls along a sequence's live slots and is 0 at its last live slot and beyond. Slots 0 to dec_lengths[b] - 1 of sequence b are live; some sequence has exactly 2048.
All inputs are finite; a program needn't handle non-finite values.
Results may differ from a plain program's by a relative error of at most 0.015.
Values may be sent and summed in bfloat16 or wider, within the bound.
A program may use at most 64 MiB of HBM per device.

v0:
```python
import math
import jax
import jax.numpy as jnp
from jax import lax
from jax.sharding import PartitionSpec as P

norm_eps = 1e-05


def from_everyone(shard, axis):
    devices = lax.axis_size(axis)
    return lax.all_to_all(
        jnp.broadcast_to(shard[None], (devices, *shard.shape)), axis, 0, 0, tiled=True
    )


def folded_in_pairs(pieces, combine):
    while len(jax.tree.leaves(pieces)[0]) > 1:
        pieces = jax.vmap(combine)(*(pieces[side::2] for side in (0, 1)))
    return pieces[0]


def prefix(shard, axis, combine, identity):
    devices, mine = (lax.axis_size(axis), lax.axis_index(axis))
    passed = jnp.arange(devices) < mine

    def kept(part, zero, own):
        part = jnp.where(
            passed.reshape(-1, *(1 for _ in own.shape)), part, jnp.asarray(zero, own.dtype)
        )
        return part

    pieces = from_everyone(shard, axis)
    return folded_in_pairs(kept(pieces, identity, shard), combine)


def taken_together(shard, axis):
    everything = from_everyone(shard, axis)
    return jnp.max(everything, axis=0)


def cut_along(shard, dim, devices):
    shape = shard.shape
    parts = shard.reshape(*shape[:dim], devices, shape[dim] // devices, *shape[dim + 1 :])
    return jnp.moveaxis(parts, dim, 0)


def sent_and_summed(shard, axis, dim):
    devices = lax.axis_size(axis)
    parts = lax.all_to_all(cut_along(shard, dim, devices), axis, 0, 0, tiled=True)
    return jnp.sum(parts.astype(jnp.float32), axis=0)


def sent_and_summed_2(shard, axis, dim):
    devices = lax.axis_size(axis)
    parts = lax.all_to_all(cut_along(shard, dim, devices), axis, 0, 0, tiled=True)
    return jnp.sum(parts, axis=0)


def sent_together(arrays, axis, dim, along):
    both = jnp.concatenate(arrays, axis=along)
    result, at, finished = (lax.all_gather(both, axis, axis=dim, tiled=True), 0, [])
    for a in arrays:
        finished.append(lax.slice_in_dim(result, at, at + a.shape[along], axis=along))
        at += a.shape[along]
    return tuple(finished)


def rms_norm(tokens, norm_gain):
    values = tokens.astype(jnp.float32)
    factor = lax.rsqrt(jnp.mean(values * values, axis=-1, keepdims=True) + norm_eps)
    return (values * factor * norm_gain).astype(jnp.bfloat16)


def project(tokens, norm_gain, query_weight, key_weight, value_weight, forget_weight, forget_bias):
    normed = rms_norm(tokens, norm_gain)
    queries = jnp.dot(normed, query_weight, preferred_element_type=jnp.float32).astype(jnp.bfloat16)
    key_rows = jnp.dot(normed, key_weight, preferred_element_type=jnp.float32).astype(jnp.bfloat16)
    value_rows = jnp.dot(normed, value_weight, preferred_element_type=jnp.float32).astype(
        jnp.bfloat16
    )
    log_gates = jax.nn.log_sigmoid(
        jnp.dot(normed, forget_weight, preferred_element_type=jnp.float32) + forget_bias
    )
    return (queries, key_rows, value_rows, log_gates)


def add_pair(earlier_sum, later_sum):
    return earlier_sum + later_sum


def shards(
    piece_tokens,
    dec_tokens,
    norm_gain,
    query_weight,
    key_weight,
    value_weight,
    forget_weight,
    forget_bias,
    out_weight,
    cache_keys,
    cache_values,
    cache_gates,
    dec_keys,
    dec_values,
    dec_gates,
    dec_lengths,
):
    piece_count = piece_tokens.shape[0]
    local_heads = forget_weight.shape[1]
    head_size = query_weight.shape[1] // local_heads
    score_scale = head_size ** (-0.5)
    piece_parts = project(
        piece_tokens, norm_gain, query_weight, key_weight, value_weight, forget_weight, forget_bias
    )
    dec_parts = project(
        dec_tokens, norm_gain, query_weight, key_weight, value_weight, forget_weight, forget_bias
    )
    piece_queries, piece_keys, piece_values, piece_gates = piece_parts
    dec_queries, dec_new_keys, dec_new_values, dec_gate_now = dec_parts
    running = jnp.cumsum(piece_gates, axis=0)
    offset = prefix(running[-1], "kv", add_pair, jnp.zeros_like(running[-1]))
    piece_bias = -(running + offset[None, :]).T
    all_queries = lax.all_gather(piece_queries, "kv", axis=0, tiled=True)
    shard_index = lax.axis_index("kv")
    key_order = shard_index * piece_count + jnp.arange(piece_count, dtype=jnp.int32)
    cache_rows = cache_keys.shape[0]
    cache_key_heads = cache_keys.reshape(cache_rows, local_heads, head_size)
    cache_value_heads = cache_values.reshape(cache_rows, local_heads, head_size)
    piece_key_heads = piece_keys.reshape(piece_count, local_heads, head_size)
    piece_value_heads = piece_values.reshape(piece_count, local_heads, head_size)
    total_rows = all_queries.shape[0]
    block_rows = math.gcd(total_rows, 512)
    block_count = total_rows // block_rows
    query_blocks = all_queries.reshape(block_count, block_rows, local_heads, head_size)
    block_starts = jnp.arange(block_count, dtype=jnp.int32) * block_rows

    def block_terms(inputs):
        query_block, first_row = inputs
        cache_scores = (
            jnp.einsum(
                "qhd,khd->hqk", query_block, cache_key_heads, preferred_element_type=jnp.float32
            )
            * score_scale
            + cache_gates[:, None, :]
        )
        piece_scores = (
            jnp.einsum(
                "qhd,khd->hqk", query_block, piece_key_heads, preferred_element_type=jnp.float32
            )
            * score_scale
            + piece_bias[:, None, :]
        )
        query_order = first_row + jnp.arange(block_rows, dtype=jnp.int32)
        visible = key_order[None, :] <= query_order[:, None]
        piece_scores = jnp.where(visible[None], piece_scores, -jnp.inf)
        local_max = jnp.maximum(jnp.max(cache_scores, axis=-1), jnp.max(piece_scores, axis=-1))
        cache_exp = jnp.exp(cache_scores - local_max[:, :, None])
        piece_exp = jnp.exp(piece_scores - local_max[:, :, None])
        numerator = jnp.einsum(
            "hqk,khd->qhd",
            cache_exp.astype(jnp.bfloat16),
            cache_value_heads,
            preferred_element_type=jnp.float32,
        )
        numerator = numerator + jnp.einsum(
            "hqk,khd->qhd",
            piece_exp.astype(jnp.bfloat16),
            piece_value_heads,
            preferred_element_type=jnp.float32,
        )
        denominator = jnp.sum(cache_exp, axis=-1) + jnp.sum(piece_exp, axis=-1)
        return (numerator.astype(jnp.bfloat16), denominator.T, local_max.T)

    numerators, denominators, local_maxima = lax.map(block_terms, (query_blocks, block_starts))
    numerators = numerators.reshape(total_rows, local_heads, head_size)
    denominators = denominators.reshape(total_rows, local_heads)
    local_maxima = local_maxima.reshape(total_rows, local_heads)
    maxima = taken_together(local_maxima, "kv")
    factors = jnp.exp(local_maxima - maxima)
    scaled = (numerators.astype(jnp.float32) * factors[:, :, None]).astype(jnp.bfloat16)
    rounded = (
        lax.optimization_barrier(scaled)
        .astype(jnp.float32)
        .reshape(total_rows, local_heads * head_size)
    )
    denominators = denominators * factors
    own_numer = sent_and_summed(rounded.astype(jnp.bfloat16), "kv", 0)
    own_denom = sent_and_summed_2(denominators, "kv", 0)
    piece_attention = (
        own_numer.reshape(piece_count, local_heads, head_size) / own_denom[:, :, None]
    ).astype(jnp.bfloat16)
    piece_attention = piece_attention.reshape(piece_count, local_heads * head_size)
    dec_count = dec_tokens.shape[0]
    dec_span = dec_keys.shape[1]
    dec_query_heads = dec_queries.reshape(dec_count, local_heads, head_size)
    new_key_heads = dec_new_keys.reshape(dec_count, local_heads, head_size)
    new_value_heads = dec_new_values.reshape(dec_count, local_heads, head_size)
    dec_key_heads = dec_keys.reshape(dec_count, dec_span, local_heads, head_size)
    dec_value_heads = dec_values.reshape(dec_count, dec_span, local_heads, head_size)
    cached = (
        jnp.einsum(
            "bhd,bkhd->bhk", dec_query_heads, dec_key_heads, preferred_element_type=jnp.float32
        )
        * score_scale
    )
    cached = cached + dec_gates + dec_gate_now[:, :, None]
    live_slots = jnp.arange(dec_span, dtype=jnp.int32)[None, :] < dec_lengths[:, None]
    cached = jnp.where(live_slots[:, None, :], cached, -jnp.inf)
    own_score = (
        jnp.sum(dec_query_heads.astype(jnp.float32) * new_key_heads.astype(jnp.float32), axis=-1)
        * score_scale
    )
    row_top = jnp.maximum(jnp.max(cached, axis=-1), own_score)
    cached_exp = jnp.exp(cached - row_top[:, :, None])
    own_exp = jnp.exp(own_score - row_top)
    whole_sum = jnp.sum(cached_exp, axis=-1) + own_exp
    cached_weights = (cached_exp / whole_sum[:, :, None]).astype(jnp.bfloat16)
    own_weights = (own_exp / whole_sum).astype(jnp.bfloat16)
    dec_mixed = jnp.einsum(
        "bhk,bkhd->bhd", cached_weights, dec_value_heads, preferred_element_type=jnp.float32
    )
    dec_mixed = dec_mixed + own_weights.astype(jnp.float32)[:, :, None] * new_value_heads.astype(
        jnp.float32
    )
    dec_attention = dec_mixed.astype(jnp.bfloat16).reshape(dec_count, local_heads * head_size)

    def add_columns(columns_in):
        return jnp.dot(columns_in, out_weight, preferred_element_type=jnp.float32)

    column_pair = sent_together((piece_attention, dec_attention), "tp", 1, 0)
    piece_out = add_columns(column_pair[0])
    dec_out = add_columns(column_pair[1])
    return (piece_out.astype(jnp.bfloat16), dec_out.astype(jnp.bfloat16), piece_keys, piece_values)


def solution(mesh):
    return jax.shard_map(
        shards,
        mesh=mesh,
        in_specs=(
            P(("grp", "kv"), None),
            P(("grp", "kv"), None),
            P(),
            P(None, "tp"),
            P(None, "tp"),
            P(None, "tp"),
            P(None, "tp"),
            P("tp"),
            P(None, "tp"),
            P(("grp", "kv"), "tp"),
            P(("grp", "kv"), "tp"),
            P("tp", ("grp", "kv")),
            P(("grp", "kv"), None, "tp"),
            P(("grp", "kv"), None, "tp"),
            P(("grp", "kv"), "tp", None),
            P(("grp", "kv")),
        ),
        out_specs=(
            P(("grp", "kv"), "tp"),
            P(("grp", "kv"), "tp"),
            P(("grp", "kv"), "tp"),
            P(("grp", "kv"), "tp"),
        ),
        check_vma=False,
    )
```

profile of v0, /device:TPU:161, one launch (start us, length us, event | category | flops | bytes accessed | tf_op | source)
XLA Modules:
  0.0 275.4 jit_solution(3541225993187929004)
XLA Ops:
  9.0 2.5 convolution_convert_fusion.3
  16.5 22.4 %all-to-all-start = ((f32[16,1,1]{2,1,0:T(1,128)}), f32[16,1,1]{2,1,0:T(1,128)S(1)}, u32[]{:S(2)}, u32[]{:S(2)}) async-start(f32[16,1,1]{2,1,0:T(1,128)} %broadcast_in_dim.35), calls=%async_computation | async-start | bytes 16384 | tf_op jit(solution)/shard_map/all_to_all | solution.py:12
  42.8 6.4 %all-to-all-done = f32[16,1,1]{2,1,0:T(1,128)S(1)} async-done(((f32[16,1,1]{2,1,0:T(1,128)}), f32[16,1,1]{2,1,0:T(1,128)S(1)}, u32[]{:S(2)}, u32[]{:S(2)}) %all-to-all-start) | async-done | bytes 96 | tf_op jit(solution)/shard_map/all_to_all | solution.py:12
  51.8 31.0 %all-gather.2.cloned.1.call-done = bf16[4096,128]{1,0:T(8,128)(2,1)} async-done(((bf16[256,128]{1,0:T(8,128)(2,1)}), bf16[4096,128]{1,0:T(8,128)(2,1)}) %all-gather.2.cloned.1.call-update) | async-done | bytes 1048592 | tf_op jit(solution)/shard_map/all_gather | solution.py:125
  82.8 76.6 %while.15 = (s32[]{:T(128)}, bf16[8,512,1,128]{3,1,2,0:T(8,128)(2,1)}, f32[8,512,1]{1,2,0:T(1,128)S(1)}, f32[8,512,1]{1,2,0:T(1,128)S(1)}, bf16[8,512,1,128]{3,1...) while((s32[]{:T(128)}, ...), condition=%wide.region_8.9_spmd.clone, body=%wide.region_3.8_spmd.clone.sunk | while | flops 1165229824 | bytes 34173624 | solution.py:176
  85.2 2.2 fusion.96
  94.8 2.2 fusion.96
  97.1 2.1 fusion.100
  104.4 2.2 fusion.96
  106.7 2.1 fusion.100
  114.0 2.2 fusion.96
  116.2 2.1 fusion.100
  123.6 2.2 fusion.96
  125.8 2.1 fusion.100
  133.1 2.2 fusion.96
  142.7 2.2 fusion.96
  152.3 2.2 fusion.96
  159.7 22.1 %all_to_all.24 = f32[16,4096,1]{1,2,0:T(1,128)S(1)} all-to-all(f32[16,4096,1]{1,2,0:T(1,128)S(1)} %broadcast_in_dim.37), channel_id=1, replica_groups=mesh['grp'=2,'kv'=16,'tp'=8] {'kv'}, dimensions={0} | all-to-all | bytes 524288 | tf_op jit(solution)/shard_map/all_to_all | solution.py:12
  182.6 4.2 %all-to-all-start.3 = ((f32[16,256,1]{1,2,0:T(1,128)}), f32[16,256,1]{1,2,0:T(1,128)S(1)}, u32[]{:S(2)}, u32[]{:S(2)}) async-start(f32[16,256,1]{1,2,0:T(1,128)} %bitcast.104), calls=%async_computation.3 | async-start | bytes 32768 | tf_op jit(solution)/shard_map/all_to_all | solution.py:56
  186.8 2.6 fusion.31
  189.4 7.8 %all-to-all-done.3 = f32[16,256,1]{1,2,0:T(1,128)S(1)} async-done(((f32[16,256,1]{1,2,0:T(1,128)}), f32[16,256,1]{1,2,0:T(1,128)S(1)}, u32[]{:S(2)}, u32[]{:S(2)}) %all-to-all-start.3) | async-done | bytes 16416 | tf_op jit(solution)/shard_map/all_to_all | solution.py:56
  197.2 4.5 %all-to-all-start.2 = ((bf16[16,256,128]{2,1,0:T(8,128)(2,1)}), bf16[16,256,128]{2,1,0:T(8,128)(2,1)S(1)}, u32[]{:S(2)}, u32[]{:S(2)}) async-start(bf16[16,256,128]{2,1,0:T(8,128)(2,1)} %bitcast.18), calls=%async_computation.2 | async-start | bytes 2097152 | tf_op jit(solution)/shard_map/all_to_all | solution.py:50
  206.8 28.7 %all-to-all-done.2 = bf16[16,256,128]{2,1,0:T(8,128)(2,1)S(1)} async-done(((bf16[16,256,128]{2,1,0:T(8,128)(2,1)}), bf16[16,256,128]{2,1,0:T(8,128)(2,1)S(1)}, u32[]{:S(2)}, u32[]{:S(2)}) %all-to-all-start.2) | async-done | bytes 1048608 | tf_op jit(solution)/shard_map/all_to_all | solution.py:50
  235.7 31.1 %all_gather.7 = bf16[260,1024]{1,0:T(8,128)(2,1)S(1)} all-gather(bf16[260,128]{1,0:T(8,128)(2,1)S(1)} %pad_maximum_fusion), channel_id=1, replica_groups=mesh['grp'=2,'kv'=16,'tp'=8] {'tp'}, dimensions={1}, use_global_device_ids=true | all-gather | bytes 599040 | tf_op jit(solution)/shard_map/all_gather | solution.py:62
  (185 shorter events, 67.9 us)
Async XLA Ops:
  7.2 197.7 %copy-start = (bf16[4,2048,128]{2,1,0:T(8,128)(2,1)S(1)}, bf16[4,2048,128]{2,1,0:T(8,128)(2,1)}, u32[]{:S(2)}) copy-start(bf16[4,2048,128]{2,1,0:T(8,128)(2,1)} %param.30) | copy-start | bytes 6291460
  7.2 5.0 %copy-start.5 = (bf16[256,2048]{1,0:T(8,128)(2,1)S(1)}, bf16[256,2048]{1,0:T(8,128)(2,1)}, u32[]{:S(2)}) copy-start(bf16[256,2048]{1,0:T(8,128)(2,1)} %param.18) | copy-start | bytes 3145732
  7.2 5.0 %copy-start.9 = (f32[2048]{0:T(1024)S(1)}, f32[2048]{0:T(1024)}, u32[]{:S(2)}) copy-start(f32[2048]{0:T(1024)} %param.20) | copy-start | bytes 24580
  7.2 5.0 %copy-start.13 = (bf16[2048,1]{0,1:T(2,128)(2,1)S(1)}, bf16[2048,1]{0,1:T(2,128)(2,1)}, u32[]{:S(2)}) copy-start(bf16[2048,1]{0,1:T(2,128)(2,1)} %param.24) | copy-start | bytes 12292
  7.2 75.6 %all-gather.2.cloned.1.call-start = ((), (), s32[]{:S(2)}) async-start(), calls=%async_computation.4 | async-start | bytes 1114112 | tf_op jit(solution)/shard_map/all_gather | solution.py:125
  16.5 32.6 %all-to-all-start = ((f32[16,1,1]{2,1,0:T(1,128)}), f32[16,1,1]{2,1,0:T(1,128)S(1)}, u32[]{:S(2)}, u32[]{:S(2)}) async-start(f32[16,1,1]{2,1,0:T(1,128)} %broadcast_in_dim.35), calls=%async_computation | async-start | bytes 16384 | tf_op jit(solution)/shard_map/all_to_all | solution.py:12
  38.9 43.9 %copy-start.1 = (bf16[4096,128]{1,0:T(8,128)(2,1)S(1)}, bf16[4096,128]{1,0:T(8,128)(2,1)}, u32[]{:S(2)}) copy-start(bf16[4096,128]{1,0:T(8,128)(2,1)} %param.27) | copy-start | bytes 3145732
  39.0 43.9 %copy-start.2 = (f32[1,4096]{1,0:T(1,128)S(1)}, f32[1,4096]{1,0:T(1,128)}, u32[]{:S(2)}) copy-start(f32[1,4096]{1,0:T(1,128)} %param.29) | copy-start | bytes 49156
  87.5 2.2 copy-start.11
  97.1 2.2 copy-start.11
  106.7 2.2 copy-start.11
  116.2 2.2 copy-start.11
  125.8 2.2 copy-start.11
  135.4 2.2 copy-start.11
  145.0 2.2 copy-start.11
  159.4 37.8 %copy-start.4 = (bf16[256,1,128]{2,0,1:T(8,128)(2,1)}, bf16[256,1,128]{2,0,1:T(8,128)(2,1)S(1)}, u32[]{:S(2)}) copy-start(bf16[256,1,128]{2,0,1:T(8,128)(2,1)S(1)} %get-tuple-element.330) | copy-start | bytes 196612
  159.4 37.8 %copy-start.14 = (bf16[256,1,128]{2,0,1:T(8,128)(2,1)}, bf16[256,1,128]{2,0,1:T(8,128)(2,1)S(1)}, u32[]{:S(2)}) copy-start(bf16[256,1,128]{2,0,1:T(8,128)(2,1)S(1)} %get-tuple-element.336) | copy-start | bytes 196612
  182.6 14.7 %all-to-all-start.3 = ((f32[16,256,1]{1,2,0:T(1,128)}), f32[16,256,1]{1,2,0:T(1,128)S(1)}, u32[]{:S(2)}, u32[]{:S(2)}) async-start(f32[16,256,1]{1,2,0:T(1,128)} %bitcast.104), calls=%async_computation.3 | async-start | bytes 32768 | tf_op jit(solution)/shard_map/all_to_all | solution.py:56
  186.8 15.0 %copy-start.7 = (bf16[4,2048]{1,0:T(4,128)(2,1)S(1)}, bf16[4,2048]{1,0:T(4,128)(2,1)}, u32[]{:S(2)}) copy-start(bf16[4,2048]{1,0:T(4,128)(2,1)} %param.19) | copy-start | bytes 49156
  197.2 38.2 %all-to-all-start.2 = ((bf16[16,256,128]{2,1,0:T(8,128)(2,1)}), bf16[16,256,128]{2,1,0:T(8,128)(2,1)S(1)}, u32[]{:S(2)}, u32[]{:S(2)}) async-start(bf16[16,256,128]{2,1,0:T(8,128)(2,1)} %bitcast.18), calls=%async_computation.2 | async-start | bytes 2097152 | tf_op jit(solution)/shard_map/all_to_all | solution.py:50
  201.8 3.8 %copy-start.8 = (f32[4,1,2048]{2,1,0:T(1,128)S(1)}, f32[4,1,2048]{2,1,0:T(1,128)}, u32[]{:S(2)}) copy-start(f32[4,1,2048]{2,1,0:T(1,128)} %param.32) | copy-start | bytes 98308
  201.8 3.8 %copy-start.10 = (s32[4]{0:T(128)S(1)}, s32[4]{0:T(128)}, u32[]{:S(2)}) copy-start(s32[4]{0:T(128)} %param.33) | copy-start | bytes 52
  201.8 4.2 %copy-start.3 = (bf16[4,2048,128]{2,1,0:T(8,128)(2,1)S(1)}, bf16[4,2048,128]{2,1,0:T(8,128)(2,1)}, u32[]{:S(2)}) copy-start(bf16[4,2048,128]{2,1,0:T(8,128)(2,1)} %param.31) | copy-start | bytes 6291460
  235.5 31.3 %copy-start.6 = (bf16[1024,256]{1,0:T(8,128)(2,1)S(1)}, bf16[1024,256]{1,0:T(8,128)(2,1)}, u32[]{:S(2)}) copy-start(bf16[1024,256]{1,0:T(8,128)(2,1)} %param.26) | copy-start | bytes 1572868
  (2 other events, 3.8 us)
Sparse Core Ops, SparseCore 0:
  11.7 71.1 all-gather.1
where the time goes:
time: 276 us; the launch traced here: 275 us
  waiting for transfers between devices  73.9 us (27%)
  matrix products  61.2 us (22%)
  blocking collectives  53.2 us (19%)
  starting transfers between devices  31.2 us (11%)
  other arithmetic  29.6 us (11%)
  between operations  17.5 us (6%)
  local copies, waits for them, and re-layouts  8.29 us (3%)
    all_gather x1, blocking collectives, sent_together(): lax.all_gather(both, axis, axis=dim, tiled=True)  31.1 us
    all_gather x1, waiting for transfers between devices, shards(): all_queries = lax.all_gather(piece_queries, 'kv', axis=0, tiled=True)  31 us
    all_to_all x1, waiting for transfers between devices, sent_and_summed(): lax.all_to_all(cut_along(shard, dim, devices), axis, 0, 0, tiled=True)  28.7 us
    all_to_all x1, starting transfers between devices, from_everyone(): lax.all_to_all(jnp.broadcast_to(shard[None], (devices, *shard.shape)), ax...  22.4 us
    all_to_all x1, blocking collectives, from_everyone(): lax.all_to_all(jnp.broadcast_to(shard[None], (devices, *shard.shape)), ax...  22.1 us
    dot_general x8, matrix products, block_terms(): jnp.einsum('qhd,khd->hqk', query_block, cache_key_heads, preferred_elemen...  18 us
    reduce_sum x16, other arithmetic, block_terms(): denominator = jnp.sum(cache_exp, axis=-1) + jnp.sum(piece_exp, axis=-1)  17.4 us
    dot_general x8, matrix products, block_terms(): jnp.einsum('hqk,khd->qhd', cache_exp.astype(jnp.bfloat16), cache_value_he...  13.8 us
  transfers between devices with their start and end apart: 4, of which 4 were waited for; matrix products, arithmetic and copies ran while one was open for 6% of the time, Pallas kernels for 0%

commit v1 on v0

--- a/solution.py
+++ b/solution.py
@@ -122,7 +122,9 @@
     running = jnp.cumsum(piece_gates, axis=0)
     offset = prefix(running[-1], "kv", add_pair, jnp.zeros_like(running[-1]))
     piece_bias = -(running + offset[None, :]).T
-    all_queries = lax.all_gather(piece_queries, "kv", axis=0, tiled=True)
+    all_queries = jnp.concatenate(
+        lax.all_to_all(jnp.stack([piece_queries] * lax.axis_size("kv")), "kv", 0, 0), axis=0
+    )
     shard_index = lax.axis_index("kv")
     key_order = shard_index * piece_count + jnp.arange(piece_count, dtype=jnp.int32)
     cache_rows = cache_keys.shape[0]

time: 276 us -> 292 us (1.058); the launches traced: 275 us -> 287 us
  waiting for transfers between devices: 73.9 us -> 95.8 us
  between operations: 17.5 us -> 4.16 us
  starting transfers between devices: 31.2 us -> 38.3 us
  blocking collectives: 53.2 us -> 48.2 us
    all_to_all x0 -> x1, waiting for transfers between devices: none -> 38.9 us  [shards(): lax.all_to_all(jnp.stack([piece_queries] * lax.axis_size('kv')), 'kv', 0, 0)]
    all_gather x1 -> x0, waiting for transfers between devices: 31 us -> none  [shards(): all_queries = lax.all_gather(piece_queries, 'kv', axis=0, tiled=True)]
    all_gather x1, blocking collectives: 31.1 us -> 17.7 us  [sent_together(): lax.all_gather(both, axis, axis=dim, tiled=True)]
    all_to_all x1, waiting for transfers between devices: 28.7 us -> 40.4 us  [sent_and_summed(): lax.all_to_all(cut_along(shard, dim, devices), axis, 0, 0, tiled=True)]
    all_to_all x1, blocking collectives: 22.1 us -> 30.5 us  [from_everyone(): lax.all_to_all(jnp.broadcast_to(shard[None], (devices, *shard.shape)), ax...]
    all_to_all x0 -> x1, starting transfers between devices: none -> 5.23 us  [shards(): lax.all_to_all(jnp.stack([piece_queries] * lax.axis_size('kv')), 'kv', 0, 0)]
  transfers between devices with their start and end apart: 4 -> 4, of which waited for: 4 -> 4; matrix products, arithmetic and copies ran while one was open for 6% -> 5% of each run, Pallas kernels for 0% -> 0%
where the time goes in v1:
time: 292 us; the launch traced here: 287 us
  waiting for transfers between devices  95.8 us (33%)
  matrix products  61.5 us (21%)
  blocking collectives  48.2 us (17%)
  starting transfers between devices  38.3 us (13%)
  other arithmetic  29.4 us (10%)
  local copies, waits for them, and re-layouts  9.48 us (3%)
  between operations  4.16 us (1%)
    all_to_all x1, waiting for transfers between devices, sent_and_summed(): lax.all_to_all(cut_along(shard, dim, devices), axis, 0, 0, tiled=True)  40.4 us
    all_to_all x1, waiting for transfers between devices, shards(): lax.all_to_all(jnp.stack([piece_queries] * lax.axis_size('kv')), 'kv', 0, 0)  38.9 us
    all_to_all x1, blocking collectives, from_everyone(): lax.all_to_all(jnp.broadcast_to(shard[None], (devices, *shard.shape)), ax...  30.5 us
    all_to_all x1, starting transfers between devices, from_everyone(): lax.all_to_all(jnp.broadcast_to(shard[None], (devices, *shard.shape)), ax...  22.4 us
    dot_general x8, matrix products, block_terms(): jnp.einsum('qhd,khd->hqk', query_block, cache_key_heads, preferred_elemen...  18.1 us
    all_gather x1, blocking collectives, sent_together(): lax.all_gather(both, axis, axis=dim, tiled=True)  17.7 us
    reduce_sum x16, other arithmetic, block_terms(): denominator = jnp.sum(cache_exp, axis=-1) + jnp.sum(piece_exp, axis=-1)  17.3 us
    dot_general x8, matrix products, block_terms(): jnp.einsum('hqk,khd->qhd', cache_exp.astype(jnp.bfloat16), cache_value_he...  13.8 us
  transfers between devices with their start and end apart: 4, of which 4 were waited for; matrix products, arithmetic and copies ran while one was open for 5% of the time, Pallas kernels for 0%

profile of v1, /device:TPU:161, one launch (start us, length us, event | category | flops | bytes accessed | tf_op | source)
XLA Modules:
  0.0 287.3 jit_solution(6876971795829406983)
XLA Ops:
  8.6 22.4 %all-to-all-start.1 = ((f32[16,1,1]{2,1,0:T(1,128)}), f32[16,1,1]{2,1,0:T(1,128)S(1)}, u32[]{:S(2)}, u32[]{:S(2)}) async-start(f32[16,1,1]{2,1,0:T(1,128)} %broadcast_in_dim.35), calls=%async_computation.1 | async-start | bytes 16384 | tf_op jit(solution)/shard_map/all_to_all | solution.py:12
  32.5 8.6 %all-to-all-done.1 = f32[16,1,1]{2,1,0:T(1,128)S(1)} async-done(((f32[16,1,1]{2,1,0:T(1,128)}), f32[16,1,1]{2,1,0:T(1,128)S(1)}, u32[]{:S(2)}, u32[]{:S(2)}) %all-to-all-start.1) | async-done | bytes 96 | tf_op jit(solution)/shard_map/all_to_all | solution.py:12
  42.3 5.2 %all-to-all-start = ((bf16[16,256,128]{2,1,0:T(8,128)(2,1)}), bf16[16,256,128]{2,1,0:T(8,128)(2,1)}, u32[]{:S(2)}, u32[]{:S(2)}) async-start(bf16[16,256,128]{2,1,0:T(8,128)(2,1)} %stack.2), calls=%async_computation | async-start | bytes 2097152 | tf_op jit(solution)/shard_map/all_to_all | solution.py:126
  54.1 38.9 %all-to-all-done = bf16[16,256,128]{2,1,0:T(8,128)(2,1)} async-done(((bf16[16,256,128]{2,1,0:T(8,128)(2,1)}), bf16[16,256,128]{2,1,0:T(8,128)(2,1)}, u32[]{:S(2)}, u32[]{:S(2)}) %all-to-all-start) | async-done | bytes 1048608 | tf_op jit(solution)/shard_map/all_to_all | solution.py:126
  93.1 76.5 %while.15 = (s32[]{:T(128)}, bf16[8,512,1,128]{3,1,2,0:T(8,128)(2,1)}, f32[8,512,1]{1,2,0:T(1,128)S(1)}, f32[8,512,1]{1,2,0:T(1,128)S(1)}, bf16[8,512,1,128]{3,1...) while((s32[]{:T(128)}, ...), condition=%wide.region_8.9_spmd.clone, body=%wide.region_3.8_spmd.clone.sunk | while | flops 1165229824 | bytes 34173624 | solution.py:178
  95.5 2.3 fusion.96
  97.8 2.1 fusion.100
  105.0 2.3 fusion.96
  107.3 2.1 fusion.100
  114.6 2.3 fusion.96
  124.2 2.3 fusion.96
  133.8 2.3 fusion.96
  136.0 2.1 fusion.100
  143.3 2.3 fusion.96
  152.9 2.3 fusion.96
  155.2 2.1 fusion.100
  162.5 2.3 fusion.96
  169.8 30.5 %all_to_all.29 = f32[16,4096,1]{1,2,0:T(1,128)S(1)} all-to-all(f32[16,4096,1]{1,2,0:T(1,128)S(1)} %broadcast_in_dim.37), channel_id=1, replica_groups=mesh['grp'=2,'kv'=16,'tp'=8] {'kv'}, dimensions={0} | all-to-all | bytes 524288 | tf_op jit(solution)/shard_map/all_to_all | solution.py:12
  201.1 6.2 %all-to-all-start.4 = ((f32[16,256,1]{1,2,0:T(1,128)}), f32[16,256,1]{1,2,0:T(1,128)S(1)}, u32[]{:S(2)}, u32[]{:S(2)}) async-start(f32[16,256,1]{1,2,0:T(1,128)} %bitcast.104), calls=%async_computation.4 | async-start | bytes 32768 | tf_op jit(solution)/shard_map/all_to_all | solution.py:56
  207.3 2.5 fusion.31
  209.9 7.8 %all-to-all-done.4 = f32[16,256,1]{1,2,0:T(1,128)S(1)} async-done(((f32[16,256,1]{1,2,0:T(1,128)}), f32[16,256,1]{1,2,0:T(1,128)S(1)}, u32[]{:S(2)}, u32[]{:S(2)}) %all-to-all-start.4) | async-done | bytes 16416 | tf_op jit(solution)/shard_map/all_to_all | solution.py:56
  217.7 4.5 %all-to-all-start.3 = ((bf16[16,256,128]{2,1,0:T(8,128)(2,1)}), bf16[16,256,128]{2,1,0:T(8,128)(2,1)S(1)}, u32[]{:S(2)}, u32[]{:S(2)}) async-start(bf16[16,256,128]{2,1,0:T(8,128)(2,1)} %bitcast.18), calls=%async_computation.3 | async-start | bytes 2097152 | tf_op jit(solution)/shard_map/all_to_all | solution.py:50
  227.2 40.4 %all-to-all-done.3 = bf16[16,256,128]{2,1,0:T(8,128)(2,1)S(1)} async-done(((bf16[16,256,128]{2,1,0:T(8,128)(2,1)}), bf16[16,256,128]{2,1,0:T(8,128)(2,1)S(1)}, u32[]{:S(2)}, u32[]{:S(2)}) %all-to-all-start.3) | async-done | bytes 1048608 | tf_op jit(solution)/shard_map/all_to_all | solution.py:50
  267.9 17.7 %all_gather.3 = bf16[260,1024]{1,0:T(8,128)(2,1)S(1)} all-gather(bf16[260,128]{1,0:T(8,128)(2,1)S(1)} %pad_maximum_fusion), channel_id=1, replica_groups=mesh['grp'=2,'kv'=16,'tp'=8] {'tp'}, dimensions={1}, use_global_device_ids=true | all-gather | bytes 599040 | tf_op jit(solution)/shard_map/all_gather | solution.py:62
  (185 shorter events, 71.6 us)
Async XLA Ops:
  0.6 224.7 %copy-start = (bf16[4,2048,128]{2,1,0:T(8,128)(2,1)S(1)}, bf16[4,2048,128]{2,1,0:T(8,128)(2,1)}, u32[]{:S(2)}) copy-start(bf16[4,2048,128]{2,1,0:T(8,128)(2,1)} %param.30) | copy-start | bytes 6291460
  0.6 30.3 %copy-start.5 = (bf16[256,2048]{1,0:T(8,128)(2,1)S(1)}, bf16[256,2048]{1,0:T(8,128)(2,1)}, u32[]{:S(2)}) copy-start(bf16[256,2048]{1,0:T(8,128)(2,1)} %param.18) | copy-start | bytes 3145732
  0.7 30.3 %copy-start.9 = (f32[2048]{0:T(1024)S(1)}, f32[2048]{0:T(1024)}, u32[]{:S(2)}) copy-start(f32[2048]{0:T(1024)} %param.20) | copy-start | bytes 24580
  8.6 32.6 %all-to-all-start.1 = ((f32[16,1,1]{2,1,0:T(1,128)}), f32[16,1,1]{2,1,0:T(1,128)S(1)}, u32[]{:S(2)}, u32[]{:S(2)}) async-start(f32[16,1,1]{2,1,0:T(1,128)} %broadcast_in_dim.35), calls=%async_computation.1 | async-start | bytes 16384 | tf_op jit(solution)/shard_map/all_to_all | solution.py:12
  42.3 50.7 %all-to-all-start = ((bf16[16,256,128]{2,1,0:T(8,128)(2,1)}), bf16[16,256,128]{2,1,0:T(8,128)(2,1)}, u32[]{:S(2)}, u32[]{:S(2)}) async-start(bf16[16,256,128]{2,1,0:T(8,128)(2,1)} %stack.2), calls=%async_computation | async-start | bytes 2097152 | tf_op jit(solution)/shard_map/all_to_all | solution.py:126
  47.6 45.5 %copy-start.1 = (bf16[4096,128]{1,0:T(8,128)(2,1)S(1)}, bf16[4096,128]{1,0:T(8,128)(2,1)}, u32[]{:S(2)}) copy-start(bf16[4096,128]{1,0:T(8,128)(2,1)} %param.27) | copy-start | bytes 3145732
  47.6 45.5 %copy-start.2 = (f32[1,4096]{1,0:T(1,128)S(1)}, f32[1,4096]{1,0:T(1,128)}, u32[]{:S(2)}) copy-start(f32[1,4096]{1,0:T(1,128)} %param.29) | copy-start | bytes 49156
  97.7 2.2 copy-start.11
  107.3 2.2 copy-start.11
  116.9 2.2 copy-start.11
  126.5 2.2 copy-start.11
  136.0 2.2 copy-start.11
  145.6 2.2 copy-start.11
  164.7 2.2 copy-start.11
  169.6 48.1 %copy-start.4 = (bf16[256,1,128]{2,0,1:T(8,128)(2,1)}, bf16[256,1,128]{2,0,1:T(8,128)(2,1)S(1)}, u32[]{:S(2)}) copy-start(bf16[256,1,128]{2,0,1:T(8,128)(2,1)S(1)} %get-tuple-element.329) | copy-start | bytes 196612
  169.6 48.1 %copy-start.14 = (bf16[256,1,128]{2,0,1:T(8,128)(2,1)}, bf16[256,1,128]{2,0,1:T(8,128)(2,1)S(1)}, u32[]{:S(2)}) copy-start(bf16[256,1,128]{2,0,1:T(8,128)(2,1)S(1)} %get-tuple-element.332) | copy-start | bytes 196612
  201.1 16.6 %all-to-all-start.4 = ((f32[16,256,1]{1,2,0:T(1,128)}), f32[16,256,1]{1,2,0:T(1,128)S(1)}, u32[]{:S(2)}, u32[]{:S(2)}) async-start(f32[16,256,1]{1,2,0:T(1,128)} %bitcast.104), calls=%async_computation.4 | async-start | bytes 32768 | tf_op jit(solution)/shard_map/all_to_all | solution.py:56
  207.3 15.0 %copy-start.7 = (bf16[4,2048]{1,0:T(4,128)(2,1)S(1)}, bf16[4,2048]{1,0:T(4,128)(2,1)}, u32[]{:S(2)}) copy-start(bf16[4,2048]{1,0:T(4,128)(2,1)} %param.19) | copy-start | bytes 49156
  209.9 15.4 %copy-start.13 = (bf16[2048,1]{0,1:T(2,128)(2,1)S(1)}, bf16[2048,1]{0,1:T(2,128)(2,1)}, u32[]{:S(2)}) copy-start(bf16[2048,1]{0,1:T(2,128)(2,1)} %param.24) | copy-start | bytes 12292
  217.7 49.9 %all-to-all-start.3 = ((bf16[16,256,128]{2,1,0:T(8,128)(2,1)}), bf16[16,256,128]{2,1,0:T(8,128)(2,1)S(1)}, u32[]{:S(2)}, u32[]{:S(2)}) async-start(bf16[16,256,128]{2,1,0:T(8,128)(2,1)} %bitcast.18), calls=%async_computation.3 | async-start | bytes 2097152 | tf_op jit(solution)/shard_map/all_to_all | solution.py:50
  222.3 3.8 %copy-start.8 = (f32[4,1,2048]{2,1,0:T(1,128)S(1)}, f32[4,1,2048]{2,1,0:T(1,128)}, u32[]{:S(2)}) copy-start(f32[4,1,2048]{2,1,0:T(1,128)} %param.32) | copy-start | bytes 98308
  222.3 3.8 %copy-start.10 = (s32[4]{0:T(128)S(1)}, s32[4]{0:T(128)}, u32[]{:S(2)}) copy-start(s32[4]{0:T(128)} %param.33) | copy-start | bytes 52
  222.3 4.2 %copy-start.3 = (bf16[4,2048,128]{2,1,0:T(8,128)(2,1)S(1)}, bf16[4,2048,128]{2,1,0:T(8,128)(2,1)}, u32[]{:S(2)}) copy-start(bf16[4,2048,128]{2,1,0:T(8,128)(2,1)} %param.31) | copy-start | bytes 6291460
  267.6 18.0 %copy-start.6 = (bf16[1024,256]{1,0:T(8,128)(2,1)S(1)}, bf16[1024,256]{1,0:T(8,128)(2,1)}, u32[]{:S(2)}) copy-start(bf16[1024,256]{1,0:T(8,128)(2,1)} %param.26) | copy-start | bytes 1572868
  (2 other events, 3.8 us)
